TPU v7x, 512 devices: a whole 4x4x16 slice. The times are simulated.
512 devices in a mesh: dp: 4 (over x), kv: 64 (over z, y), tp: 2 (over core).
Axes of the slice: x: 4, y: 4, z: 16, core: 2. Of those that a mesh axis runs over, the one named last changes fastest.
Arguments:
- tokens: bfloat16 [768, 2048], P('dp', ('kv', 'tp')), may hold values from -21 to 21
- state: float32 [768, 8, 128, 128], P(('dp', 'kv'), 'tp'), may hold values from -3 to 3
- mix_gain: bfloat16 [2048], P(('kv', 'tp')), may hold values from 0.099609375 to 1.8984375
- w_query: bfloat16 [2048, 1024], P('kv', 'tp'), may hold values from -0.125 to 0.125
- w_key: bfloat16 [2048, 1024], P('kv', 'tp'), may hold values from -0.125 to 0.125
- w_value: bfloat16 [2048, 1024], P('kv', 'tp'), may hold values from -0.125 to 0.125
- w_beta: bfloat16 [2048, 8], P('kv', 'tp'), may hold values from -0.125 to 0.125
- w_decay: bfloat16 [2048, 8], P('kv', 'tp'), may hold values from -0.125 to 0.125
- decay_log: float32 [8], P('tp'), may hold values from -1.5 to 1
- head_gain: bfloat16 [128], replicated, may hold values from 0.099609375 to 1.8984375
- w_out: bfloat16 [1024, 2048], P('tp', 'kv'), may hold values from -0.1875 to 0.1875
- ff_gain: bfloat16 [2048], P(('kv', 'tp')), may hold values from 0.099609375 to 1.8984375
- w_up: bfloat16 [2048, 8192], P(None, ('kv', 'tp')), may hold values from -0.125 to 0.125
- w_down: bfloat16 [8192, 2048], P(('kv', 'tp')), may hold values from -0.25 to 0.25
Outputs:
- output: bfloat16 [768, 2048], P('dp', ('kv', 'tp'))
- new_state: float32 [768, 8, 128, 128], P(('dp', 'kv'), 'tp')
All inputs are finite; a program needn't handle non-finite values.
Results may differ from a plain program's by a relative error of at most 0.013.
Values may be sent and summed in bfloat16 or wider, within the bound.
A program may use at most 64 MiB of HBM per device.

v0:
```python
import math
import jax
import jax.numpy as jnp
from jax import lax
from jax.sharding import PartitionSpec as P

D = 2048


def gather_turned(arrays, axis, dims):
    turned = [jnp.moveaxis(a, dim, 0) for a, dim in zip(arrays, dims)]
    both = jnp.concatenate([t.reshape(len(t), -1) for t in turned], axis=1)
    filled, at, finished = (lax.all_gather(both, axis, axis=0, tiled=True), 0, [])
    for t, dim in zip(turned, dims):
        slab = filled[:, at : at + t[0].size].reshape(-1, *t.shape[1:])
        finished.append(jnp.moveaxis(slab, 0, dim))
        at += t[0].size
    return tuple(finished)


def in_blocks(value, dim, size):
    before, after = (value.shape[:dim], value.shape[dim + 1 :])
    return jnp.moveaxis(value.reshape(*before, size, -1, *after), dim, 0)


def sent_and_summed(value, axis, dim):
    size = lax.axis_size(axis)
    pieces = lax.all_to_all(in_blocks(value, dim, size), axis, 0, 0, tiled=True)
    return jnp.sum(pieces.astype(jnp.float32), axis=0)


def in_one_piece(arrays, axis, dim, along):
    widths = [math.prod(a.shape[along:]) for a in arrays]
    both = jnp.concatenate(
        [a.reshape(*a.shape[:along], w) for a, w in zip(arrays, widths)], axis=along
    )
    filled = sent_and_summed(both, axis, dim)
    pieces = jnp.split(filled, [sum(widths[:k]) for k in range(1, len(widths))], axis=along)
    return tuple(
        (b.reshape(*filled.shape[:along], *a.shape[along:]) for a, b in zip(arrays, pieces))
    )


def copy_for_each(value, axis):
    copies = jnp.broadcast_to(value, (lax.axis_size(axis), *value.shape))
    return lax.all_to_all(copies, axis, split_axis=0, concat_axis=0, tiled=True)


def in_order(pieces, dim):
    pieces = jnp.moveaxis(pieces, 0, dim)
    shape = pieces.shape
    return pieces.reshape(*shape[:dim], shape[dim] * shape[dim + 1], *shape[dim + 2 :])


def collect(value, axis, dim):
    pieces = copy_for_each(value, axis)
    return in_order(pieces, dim)


def one_gather(arrays, axis, dims):
    vector = jnp.concatenate([a.reshape(-1) for a in arrays])
    lines, at, finished = (lax.all_gather(vector, axis), 0, [])
    for a, dim in zip(arrays, dims):
        pieces = lines[:, at : at + a.size].reshape(-1, *a.shape)
        finished.append(in_order(pieces, dim))
        at += a.size
    return tuple(finished)


def local(
    tokens,
    state,
    mix_gain,
    w_query,
    w_key,
    w_value,
    w_beta,
    w_decay,
    decay_log,
    head_gain,
    w_out,
    ff_gain,
    w_up,
    w_down,
):
    seq_count = state.shape[0]
    heads_local = state.shape[1]
    head_size = state.shape[2]
    tokens_wide, gain_wide = gather_turned((tokens, mix_gain[None, :]), "tp", (1, 1))
    wide_float = tokens_wide.astype(jnp.float32)
    scaled = (wide_float * gain_wide.astype(jnp.float32)).astype(jnp.bfloat16)
    query_part = jnp.dot(scaled, w_query, preferred_element_type=jnp.float32)
    key_part = jnp.dot(scaled, w_key, preferred_element_type=jnp.float32)
    value_part = jnp.dot(scaled, w_value, preferred_element_type=jnp.float32)
    gate_part = jnp.concatenate(
        [
            jnp.dot(scaled, w_beta, preferred_element_type=jnp.float32),
            jnp.dot(scaled, w_decay, preferred_element_type=jnp.float32),
        ],
        axis=1,
    )
    square_part = jnp.sum(wide_float * wide_float, axis=1)
    query_sum, key_sum, value_sum, gate_sum, square_sum = in_one_piece(
        (
            query_part.astype(jnp.bfloat16),
            key_part.astype(jnp.bfloat16),
            value_part.astype(jnp.bfloat16),
            gate_part.astype(jnp.bfloat16),
            square_part.astype(jnp.bfloat16),
        ),
        "kv",
        0,
        1,
    )
    inverse = lax.rsqrt(square_sum / D + 1e-06)[:, None]
    query = (inverse * query_sum).reshape(seq_count, heads_local, head_size)
    key_rows = (inverse * key_sum).reshape(seq_count, heads_local, head_size)
    value = (inverse * value_sum).reshape(seq_count, heads_local, head_size)
    gates = inverse * gate_sum
    beta = jax.nn.sigmoid(gates[:, :heads_local])
    decay = -jnp.exp(decay_log)[None, :] * jax.nn.softplus(gates[:, heads_local:])
    qnorm = query * lax.rsqrt(jnp.sum(query * query, axis=-1, keepdims=True) + 1e-06)
    knorm = key_rows * lax.rsqrt(jnp.sum(key_rows * key_rows, axis=-1, keepdims=True) + 1e-06)
    kept = state * jnp.exp(decay)[:, :, None, None]
    predicted = jnp.sum(kept * knorm[:, :, :, None], axis=2)
    new_state = (
        kept + (beta[:, :, None] * knorm)[:, :, :, None] * (value - predicted)[:, :, None, :]
    )
    heads = jnp.sum(new_state * qnorm[:, :, :, None], axis=2) / jnp.sqrt(jnp.float32(head_size))
    normed = (
        heads
        * lax.rsqrt(jnp.mean(heads * heads, axis=-1, keepdims=True) + 1e-06)
        * head_gain.astype(jnp.float32)
    )
    normed = normed.astype(jnp.bfloat16).reshape(seq_count, heads_local * head_size)
    partial_mix = jnp.dot(collect(normed, "kv", 0), w_out, preferred_element_type=jnp.float32)
    mixed = sent_and_summed(partial_mix.astype(jnp.bfloat16), "tp", 1)
    resid = (tokens.astype(jnp.float32) + mixed).astype(jnp.bfloat16)
    up_weight, down_weight, gain_pair = one_gather(
        (w_up, w_down, ff_gain[None, :]), "tp", (1, 0, 1)
    )
    gain_local = gain_pair[0]
    work_rows = lax.all_to_all(resid, "tp", split_axis=0, concat_axis=1, tiled=True)
    resid_float = work_rows.astype(jnp.float32)
    whole_rows, whole_gain = gather_turned((work_rows, gain_local[None, :]), "kv", (1, 1))
    whole_float = whole_rows.astype(jnp.float32)
    inverse2 = lax.rsqrt(jnp.mean(whole_float * whole_float, axis=1, keepdims=True) + 1e-06)
    scaled2 = (whole_float * whole_gain.astype(jnp.float32)).astype(jnp.bfloat16)
    up_rows = jnp.dot(scaled2, up_weight, preferred_element_type=jnp.float32) * inverse2
    act = jnp.square(jax.nn.relu(up_rows)).astype(jnp.bfloat16)
    summed = sent_and_summed(
        lax.dot_general(
            down_weight, act, (((0,), (1,)), ((), ())), preferred_element_type=jnp.float32
        ).astype(jnp.bfloat16),
        "kv",
        0,
    )
    results = (resid_float + summed.T).astype(jnp.bfloat16)
    output = results
    output = lax.all_to_all(output, "tp", split_axis=1, concat_axis=0, tiled=True)
    return (output, new_state)


def solution(mesh):
    placed = (
        P("dp", ("kv", "tp")),
        P(("dp", "kv"), "tp", None, None),
        P(("kv", "tp")),
        P("kv", "tp"),
        P("kv", "tp"),
        P("kv", "tp"),
        P("kv", "tp"),
        P("kv", "tp"),
        P("tp"),
        P(),
        P("tp", "kv"),
        P(("kv", "tp")),
        P(None, ("kv", "tp")),
        P(("kv", "tp"), None),
    )
    return jax.shard_map(
        local,
        mesh=mesh,
        in_specs=placed,
        out_specs=(P("dp", ("kv", "tp")), P(("dp", "kv"), "tp", None, None)),
        check_vma=False,
    )
```

profile of v0, /device:TPU:1, one launch (start us, length us, event | category | flops | bytes accessed | tf_op | source)
XLA Modules:
  0.0 285.4 jit_solution(2601442207486391683)
XLA Ops:
  7.2 0.8 copy.104
  7.9 0.8 pad_maximum_fusion.1
  8.7 8.3 %all_gather.12 = bf16[32,193]{1,0:T(8,128)(2,1)S(1)} all-gather(bf16[16,193]{1,0:T(8,128)(2,1)S(1)} %pad_maximum_fusion.1), channel_id=1, replica_groups=mesh['dp'=4,'kv'=64,'tp'=2] {'tp'}, dimensions={0}, use_global_device_ids=true | all-gather | bytes 18528 | tf_op jit(solution)/shard_map/all_gather | solution.py:13
  17.2 0.3 convolution_convert_fusion.3
  17.7 1.1 convolution_convert_fusion.2
  19.7 0.5 copy.105
  20.6 0.5 copy.106
  21.3 2.0 concatenate.33
  23.3 13.2 %all-to-all-start = ((bf16[64,3,1545]{2,1,0:T(4,128)(2,1)}), bf16[64,3,1545]{2,1,0:T(4,128)(2,1)S(1)}, u32[]{:S(2)}, u32[]{:S(2)}) async-start(bf16[64,3,1545]{2,1,0:T(4,128)(2,1)} %concatenate.33), calls=%async_computation | async-start | bytes 1703936 | tf_op jit(solution)/shard_map/all_to_all | solution.py:28
  37.3 1.3 dynamic-slice
  39.3 4.9 %dynamic-update-slice = bf16[524320]{0:T(1024)(128)(2,1)S(1)} dynamic-update-slice(bf16[524320]{0:T(1024)(128)(2,1)S(1)} %broadcast.84, bf16[262160]{0:T(1024)(128)(2,1)S(1)} %pad_maximum_fusion, u32[]{:T(128)} %bitcast.7) | dynamic-update-slice | bytes 1048644
  44.2 1.0 copy-done.1
  45.2 43.0 %all-reduce.3.cloned.1.call-done = bf16[524320]{0:T(1024)(128)(2,1)} async-done(((bf16[524320]{0:T(1024)(128)(2,1)}), bf16[524320]{0:T(1024)(128)(2,1)}) %all-reduce.3.cloned.1.call-update) | async-done | bytes 1048656
  88.2 2.6 reshape.153
  90.9 0.4 convert_reduce_fusion
  92.4 0.3 multiply_reduce_fusion.1
  92.7 1.4 multiply_reduce_fusion
  94.5 0.8 broadcast_in_dim.2
  95.2 14.4 %all-to-all-start.1 = ((bf16[64,3,512]{2,1,0:T(4,128)(2,1)}), bf16[64,3,512]{2,1,0:T(4,128)(2,1)S(1)}, u32[]{:S(2)}, u32[]{:S(2)}) async-start(bf16[64,3,512]{2,1,0:T(4,128)(2,1)} %broadcast_in_dim.2), calls=%async_computation.1 | async-start | bytes 524288 | tf_op jit(solution)/shard_map/all_to_all | solution.py:46
  109.6 0.7 fusion.28
  110.3 0.5 reshape_reshape.3
  110.8 0.7 reshape.148
  111.5 0.3 copy.117
  112.2 17.7 %all-to-all-done.1 = bf16[64,3,512]{2,1,0:T(4,128)(2,1)S(1)} async-done(((bf16[64,3,512]{2,1,0:T(4,128)(2,1)}), bf16[64,3,512]{2,1,0:T(4,128)(2,1)S(1)}, u32[]{:S(2)}, u32[]{:S(2)}) %all-to-all-start.1) | async-done | bytes 196640 | tf_op jit(solution)/shard_map/all_to_all | solution.py:46
  130.3 6.5 %all_to_all.58 = bf16[2,192,16]{1,2,0:T(8,128)(2,1)S(1)} all-to-all(bf16[2,192,16]{1,2,0:T(8,128)(2,1)S(1)} %bitcast.54), channel_id=1, replica_groups=mesh['dp'=4,'kv'=64,'tp'=2] {'tp'}, dimensions={0} | all-to-all | bytes 24576 | tf_op jit(solution)/shard_map/all_to_all | solution.py:28
  136.9 3.7 %all_to_all.59 = bf16[2,96,16]{1,2,0:T(8,128)(2,1)S(1)} all-to-all(bf16[2,96,16]{1,2,0:T(8,128)(2,1)S(1)} %copy.114), channel_id=1, replica_groups=mesh['dp'=4,'kv'=64,'tp'=2] {'tp'}, dimensions={0} | all-to-all | bytes 12288 | tf_op jit(solution)/shard_map/all_to_all | solution.py:143
  140.7 72.8 %all_gather.15 = bf16[2048,97]{1,0:T(8,128)(2,1)S(1)} all-gather(bf16[32,97]{1,0:T(8,128)(2,1)S(1)} %pad_maximum_fusion.2), channel_id=1, replica_groups=mesh['dp'=4,'kv'=64,'tp'=2] {'kv'}, dimensions={0}, use_global_device_ids=true | all-gather | bytes 403520 | tf_op jit(solution)/shard_map/all_gather | solution.py:13
  213.5 0.4 convert_reduce_fusion.1
  214.2 1.1 convolution_convert_fusion
  215.6 27.9 %all_to_all.60 = bf16[64,32,96]{2,1,0:T(8,128)(2,1)S(1)} all-to-all(bf16[64,32,96]{2,1,0:T(8,128)(2,1)S(1)} %bitcast.50), channel_id=1, replica_groups=mesh['dp'=4,'kv'=64,'tp'=2] {'kv'}, dimensions={0} | all-to-all | bytes 786432 | tf_op jit(solution)/shard_map/all_to_all | solution.py:28
  243.6 34.2 %all_to_all.61 = bf16[96,2,16]{0,2,1:T(8,128)(2,1)S(1)} all-to-all(bf16[96,2,16]{0,2,1:T(8,128)(2,1)S(1)} %bitcast.57), channel_id=1, replica_groups=mesh['dp'=4,'kv'=64,'tp'=2] {'tp'}, dimensions={1} | all-to-all | bytes 12288 | tf_op jit(solution)/shard_map/all_to_all | solution.py:160
  277.8 0.7 all_to_all.51
  (88 shorter events, 5.8 us)
Async XLA Ops:
  7.2 10.1 %copy-start = (bf16[32,512]{1,0:T(8,128)(2,1)S(1)}, bf16[32,512]{1,0:T(8,128)(2,1)}, u32[]{:S(2)}) copy-start(bf16[32,512]{1,0:T(8,128)(2,1)} %param.17) | copy-start | bytes 98308
  7.2 11.7 %copy-start.6 = (bf16[32,512]{1,0:T(8,128)(2,1)S(1)}, bf16[32,512]{1,0:T(8,128)(2,1)}, u32[]{:S(2)}) copy-start(bf16[32,512]{1,0:T(8,128)(2,1)} %param.19) | copy-start | bytes 98308
  17.2 2.1 copy-start.10
  17.5 2.6 copy-start.11
  23.3 13.3 %copy-start.5 = (bf16[64,2048]{1,0:T(8,128)(2,1)S(1)}, bf16[64,2048]{1,0:T(8,128)(2,1)}, u32[]{:S(2)}) copy-start(bf16[64,2048]{1,0:T(8,128)(2,1)} %param.27) | copy-start | bytes 786436
  23.3 13.4 %copy-start.4 = (bf16[2048,64]{0,1:T(8,128)(2,1)S(1)}, bf16[2048,64]{0,1:T(8,128)(2,1)}, u32[]{:S(2)}) copy-start(bf16[2048,64]{0,1:T(8,128)(2,1)} %param.26) | copy-start | bytes 786436
  23.3 67.6 %all-to-all-start = ((bf16[64,3,1545]{2,1,0:T(4,128)(2,1)}), bf16[64,3,1545]{2,1,0:T(4,128)(2,1)S(1)}, u32[]{:S(2)}, u32[]{:S(2)}) async-start(bf16[64,3,1545]{2,1,0:T(4,128)(2,1)} %concatenate.33), calls=%async_computation | async-start | bytes 1703936 | tf_op jit(solution)/shard_map/all_to_all | solution.py:28
  36.5 0.7 copy-start.9
  36.6 51.7 %all-reduce.3.cloned.1.call-start = ((), (), s32[]{:S(2)}) async-start(), calls=%async_computation.6 | async-start | bytes 2101248
  39.3 5.9 %copy-start.12 = (bf16[128]{0:T(256)(128)(2,1)S(1)}, bf16[128]{0:T(256)(128)(2,1)}, u32[]{:S(2)}) copy-start(bf16[128]{0:T(256)(128)(2,1)} %param.23) | copy-start | bytes 772
  39.3 5.9 %copy-start.13 = (f32[4]{0:T(128)S(1)}, f32[4]{0:T(128)}, u32[]{:S(2)}) copy-start(f32[4]{0:T(128)} %param.22) | copy-start | bytes 52
  44.2 1.0 copy-start.1
  90.8 19.5 %copy-start.2 = (bf16[2,262160]{1,0:T(2,128)(2,1)}, bf16[2,262160]{1,0:T(2,128)(2,1)S(1)}, u32[]{:S(2)}) copy-start(bf16[2,262160]{1,0:T(2,128)(2,1)S(1)} %reshape.153) | copy-start | bytes 3145924
  90.8 1.6 copy-start.3
  95.2 34.7 %all-to-all-start.1 = ((bf16[64,3,512]{2,1,0:T(4,128)(2,1)}), bf16[64,3,512]{2,1,0:T(4,128)(2,1)S(1)}, u32[]{:S(2)}, u32[]{:S(2)}) async-start(bf16[64,3,512]{2,1,0:T(4,128)(2,1)} %broadcast_in_dim.2), calls=%async_computation.1 | async-start | bytes 524288 | tf_op jit(solution)/shard_map/all_to_all | solution.py:46
  111.5 0.7 slice-start
  111.5 18.7 %copy-start.7 = (bf16[512,32]{0,1:T(8,128)(2,1)S(1)}, bf16[512,32]{0,1:T(8,128)(2,1)}, u32[]{:S(2)}) copy-start(bf16[512,32]{0,1:T(8,128)(2,1)} %param.24) | copy-start | bytes 98308
  111.5 25.3 %copy-start.8 = (bf16[192,16]{0,1:T(8,128)(2,1)S(1)}, bf16[192,16]{0,1:T(8,128)(2,1)}, u32[]{:S(2)}) copy-start(bf16[192,16]{0,1:T(8,128)(2,1)} %param.14) | copy-start | bytes 18436
Sparse Core Ops, SparseCore 0:
  45.3 42.8 all-reduce.2
where the time goes:
time: 286 us; the launch traced here: 285 us
  blocking collectives  153 us (53%)
  waiting for transfers between devices  60.7 us (21%)
  starting transfers between devices  27.6 us (10%)
  local copies, waits for them, and re-layouts  20.3 us (7%)
  between operations  15.1 us (5%)
  other arithmetic  4.86 us (2%)
  matrix products  3.28 us (1%)
    all_gather x2, blocking collectives, gather_turned(): lax.all_gather(both, axis, axis=0, tiled=True)  81.1 us
    unnamed x2, waiting for transfers between devices  43 us
    all_to_all x2, blocking collectives, sent_and_summed(): pieces = lax.all_to_all(in_blocks(value, dim, size), axis, 0, 0, tiled=True)  34.3 us
    all_to_all x1, blocking collectives, local(): lax.all_to_all(output, 'tp', split_axis=1, concat_axis=0, tiled=True)  34.2 us
    all_to_all x1, waiting for transfers between devices, copy_for_each(): return lax.all_to_all(copies, axis, split_axis=0, concat_axis=0, tiled=True)  17.7 us
    all_to_all x1, starting transfers between devices, copy_for_each(): return lax.all_to_all(copies, axis, split_axis=0, concat_axis=0, tiled=True)  14.4 us
    all_to_all x1, starting transfers between devices, sent_and_summed(): pieces = lax.all_to_all(in_blocks(value, dim, size), axis, 0, 0, tiled=True)  13.2 us
    unnamed x35, local copies, waits for them, and re-layouts  7.79 us
  transfers between devices with their start and end apart: 3, of which 2 were waited for; matrix products, arithmetic and copies ran while one was open for 4% of the time, Pallas kernels for 0%

commit v1 on v0

--- a/solution.py
+++ b/solution.py
@@ -7,10 +7,18 @@
 D = 2048
 
 
+def raise_area(tile_in, row_axis):
+    big = lax.psum(1, axis_name=row_axis)
+    v_next = jnp.stack([tile_in] * big, axis=0)
+    o_now = lax.all_to_all(v_next, row_axis, 0, 0)
+    all_values = jnp.concatenate(o_now, axis=0)
+    return all_values
+
+
 def gather_turned(arrays, axis, dims):
     turned = [jnp.moveaxis(a, dim, 0) for a, dim in zip(arrays, dims)]
     both = jnp.concatenate([t.reshape(len(t), -1) for t in turned], axis=1)
-    filled, at, finished = (lax.all_gather(both, axis, axis=0, tiled=True), 0, [])
+    filled, at, finished = (raise_area(both, axis), 0, [])
     for t, dim in zip(turned, dims):
         slab = filled[:, at : at + t[0].size].reshape(-1, *t.shape[1:])
         finished.append(jnp.moveaxis(slab, 0, dim))

time: 286 us -> 218 us (0.76)
  blocking collectives: 153 us -> 65.8 us
  waiting for transfers between devices: 60.7 us -> 80.1 us
    all_gather x2 -> x0, blocking collectives: 81.1 us -> none  [gather_turned(): lax.all_gather(both, axis, axis=0, tiled=True)]
    unnamed x2, waiting for transfers between devices: 43 us -> 0.04 us
    all_to_all x1, waiting for transfers between devices: 0.01 us -> 34.9 us  [sent_and_summed(): pieces = lax.all_to_all(in_blocks(value, dim, size), axis, 0, 0, tiled=True)]
    all_to_all x0 -> x1, waiting for transfers between devices: none -> 28.8 us  [raise_area(): o_now = lax.all_to_all(v_next, row_axis, 0, 0)]
    all_to_all x1, blocking collectives: 34.2 us -> 7.75 us  [local(): lax.all_to_all(output, 'tp', split_axis=1, concat_axis=0, tiled=True)]
    all_to_all x0 -> x1, blocking collectives: none -> 10.2 us  [raise_area(): o_now = lax.all_to_all(v_next, row_axis, 0, 0)]
    all_to_all x2, blocking collectives: 34.3 us -> 44.1 us  [sent_and_summed(): pieces = lax.all_to_all(in_blocks(value, dim, size), axis, 0, 0, tiled=True)]
    all_to_all x1, starting transfers between devices: 14.4 us -> 8.59 us  [copy_for_each(): return lax.all_to_all(copies, axis, split_axis=0, concat_axis=0, tiled=True)]
  transfers between devices with their start and end apart: 3 -> 4, of which waited for: 2 -> 3; matrix products, arithmetic and copies ran while one was open for 4% -> 7% of each run, Pallas kernels for 0% -> 0%
where the time goes in v1:
time: 218 us; the launch traced here: 217 us
  waiting for transfers between devices  80.1 us (37%)
  blocking collectives  65.8 us (30%)
  starting transfers between devices  26.7 us (12%)
  local copies, waits for them, and re-layouts  21.2 us (10%)
  between operations  15.1 us (7%)
  other arithmetic  4.69 us (2%)
  matrix products  3.28 us (2%)
    all_to_all x2, blocking collectives, sent_and_summed(): pieces = lax.all_to_all(in_blocks(value, dim, size), axis, 0, 0, tiled=True)  44.1 us
    all_to_all x1, waiting for transfers between devices, sent_and_summed(): pieces = lax.all_to_all(in_blocks(value, dim, size), axis, 0, 0, tiled=True)  34.9 us
    all_to_all x1, waiting for transfers between devices, raise_area(): o_now = lax.all_to_all(v_next, row_axis, 0, 0)  28.8 us
    all_to_all x1, waiting for transfers between devices, copy_for_each(): return lax.all_to_all(copies, axis, split_axis=0, concat_axis=0, tiled=True)  16.4 us
    all_to_all x1, starting transfers between devices, sent_and_summed(): pieces = lax.all_to_all(in_blocks(value, dim, size), axis, 0, 0, tiled=True)  13.2 us
    all_to_all x1, blocking collectives, raise_area(): o_now = lax.all_to_all(v_next, row_axis, 0, 0)  10.2 us
    all_to_all x1, starting transfers between devices, copy_for_each(): return lax.all_to_all(copies, axis, split_axis=0, concat_axis=0, tiled=True)  8.59 us
    unnamed x34, local copies, waits for them, and re-layouts  7.9 us
  transfers between devices with their start and end apart: 4, of which 3 were waited for; matrix products, arithmetic and copies ran while one was open for 7% of the time, Pallas kernels for 0%

profile of v1, /device:TPU:1, one launch (start us, length us, event | category | flops | bytes accessed | tf_op | source)
XLA Modules:
  0.0 216.9 jit_solution(10695446534793306176)
XLA Ops:
  7.2 0.8 copy.112
  7.9 0.8 maximum_bitcast_fusion
  8.7 10.2 %all_to_all.68 = bf16[2,16,193]{2,1,0:T(8,128)(2,1)S(1)} all-to-all(bf16[2,16,193]{2,1,0:T(8,128)(2,1)S(1)} %pad_maximum_fusion.1), channel_id=1, replica_groups=mesh['dp'=4,'kv'=64,'tp'=2] {'tp'}, dimensions={0} | all-to-all | bytes 24704 | tf_op jit(solution)/shard_map/all_to_all | solution.py:13
  19.6 1.1 convolution_convert_fusion.2
  21.6 0.5 copy.114
  22.5 0.5 copy.115
  23.2 2.0 concatenate.33
  25.2 13.2 %all-to-all-start.1 = ((bf16[64,3,1545]{2,1,0:T(4,128)(2,1)}), bf16[64,3,1545]{2,1,0:T(4,128)(2,1)S(1)}, u32[]{:S(2)}, u32[]{:S(2)}) async-start(bf16[64,3,1545]{2,1,0:T(4,128)(2,1)} %concatenate.33), calls=%async_computation.1 | async-start | bytes 1703936 | tf_op jit(solution)/shard_map/all_to_all | solution.py:36
  39.2 1.3 dynamic-slice
  41.2 4.9 %dynamic-update-slice = bf16[524320]{0:T(1024)(128)(2,1)S(1)} dynamic-update-slice(bf16[524320]{0:T(1024)(128)(2,1)S(1)} %broadcast.86, bf16[262160]{0:T(1024)(128)(2,1)S(1)} %pad_maximum_fusion, u32[]{:T(128)} %bitcast.10) | dynamic-update-slice | bytes 1048644
  46.2 1.0 copy-done.1
  47.2 34.9 %all-to-all-done.1 = bf16[64,3,1545]{2,1,0:T(4,128)(2,1)S(1)} async-done(((bf16[64,3,1545]{2,1,0:T(4,128)(2,1)}), bf16[64,3,1545]{2,1,0:T(4,128)(2,1)S(1)}, u32[]{:S(2)}, u32[]{:S(2)}) %all-to-all-start.1) | async-done | bytes 593312 | tf_op jit(solution)/shard_map/all_to_all | solution.py:36
  82.2 0.4 convert_reduce_fusion
  84.0 1.4 multiply_reduce_fusion
  85.8 0.8 broadcast_in_dim.2
  86.6 8.6 %all-to-all-start.2 = ((bf16[64,3,512]{2,1,0:T(4,128)(2,1)}), bf16[64,3,512]{2,1,0:T(4,128)(2,1)S(1)}, u32[]{:S(2)}, u32[]{:S(2)}) async-start(bf16[64,3,512]{2,1,0:T(4,128)(2,1)} %broadcast_in_dim.2), calls=%async_computation.2 | async-start | bytes 524288 | tf_op jit(solution)/shard_map/all_to_all | solution.py:54
  95.2 2.6 %reshape.163 = bf16[2,262160]{1,0:T(2,128)(2,1)S(1)} reshape(bf16[524320]{0:T(1024)(128)(2,1)} %all-reduce.3.cloned.1.call-done) | data formatting | bytes 2097280 | tf_op jit(solution)/shard_map/all_gather | solution.py:70
  97.9 16.4 %all-to-all-done.2 = bf16[64,3,512]{2,1,0:T(4,128)(2,1)S(1)} async-done(((bf16[64,3,512]{2,1,0:T(4,128)(2,1)}), bf16[64,3,512]{2,1,0:T(4,128)(2,1)S(1)}, u32[]{:S(2)}, u32[]{:S(2)}) %all-to-all-start.2) | async-done | bytes 196640 | tf_op jit(solution)/shard_map/all_to_all | solution.py:54
  114.7 7.9 %all_to_all.69 = bf16[2,192,16]{1,2,0:T(8,128)(2,1)S(1)} all-to-all(bf16[2,192,16]{1,2,0:T(8,128)(2,1)S(1)} %bitcast.71), channel_id=1, replica_groups=mesh['dp'=4,'kv'=64,'tp'=2] {'tp'}, dimensions={0} | all-to-all | bytes 24576 | tf_op jit(solution)/shard_map/all_to_all | solution.py:36
  122.6 3.7 %all_to_all.70 = bf16[2,96,16]{1,2,0:T(8,128)(2,1)S(1)} all-to-all(bf16[2,96,16]{1,2,0:T(8,128)(2,1)S(1)} %copy.123), channel_id=1, replica_groups=mesh['dp'=4,'kv'=64,'tp'=2] {'tp'}, dimensions={0} | all-to-all | bytes 12288 | tf_op jit(solution)/shard_map/all_to_all | solution.py:151
  126.4 0.9 stack.8
  127.3 4.8 %all-to-all-start.5 = ((bf16[64,32,97]{2,1,0:T(8,128)(2,1)}), bf16[64,32,97]{2,1,0:T(8,128)(2,1)S(1)}, u32[]{:S(2)}, u32[]{:S(2)}) async-start(bf16[64,32,97]{2,1,0:T(8,128)(2,1)} %stack.8), calls=%async_computation.5 | async-start | bytes 1048576 | tf_op jit(solution)/shard_map/all_to_all | solution.py:13
  132.1 0.7 fusion.28
  132.8 0.5 reshape_reshape.3
  133.3 0.7 reshape.158
  134.0 0.4 copy.126
  134.3 28.8 %all-to-all-done.5 = bf16[64,32,97]{2,1,0:T(8,128)(2,1)S(1)} async-done(((bf16[64,32,97]{2,1,0:T(8,128)(2,1)}), bf16[64,32,97]{2,1,0:T(8,128)(2,1)S(1)}, u32[]{:S(2)}, u32[]{:S(2)}) %all-to-all-start.5) | async-done | bytes 397344 | tf_op jit(solution)/shard_map/all_to_all | solution.py:13
  163.1 0.4 convert_reduce_fusion.1
  163.8 1.1 convolution_convert_fusion
  165.2 36.3 %all_to_all.71 = bf16[64,32,96]{2,1,0:T(8,128)(2,1)S(1)} all-to-all(bf16[64,32,96]{2,1,0:T(8,128)(2,1)S(1)} %bitcast.60), channel_id=1, replica_groups=mesh['dp'=4,'kv'=64,'tp'=2] {'kv'}, dimensions={0} | all-to-all | bytes 786432 | tf_op jit(solution)/shard_map/all_to_all | solution.py:36
  201.6 7.7 %all_to_all.72 = bf16[96,2,16]{0,2,1:T(8,128)(2,1)S(1)} all-to-all(bf16[96,2,16]{0,2,1:T(8,128)(2,1)S(1)} %bitcast.74), channel_id=1, replica_groups=mesh['dp'=4,'kv'=64,'tp'=2] {'tp'}, dimensions={1} | all-to-all | bytes 12288 | tf_op jit(solution)/shard_map/all_to_all | solution.py:168
  209.3 0.7 all_to_all.59
  (90 shorter events, 6.1 us)
Async XLA Ops:
  7.2 12.0 %copy-start = (bf16[32,512]{1,0:T(8,128)(2,1)S(1)}, bf16[32,512]{1,0:T(8,128)(2,1)}, u32[]{:S(2)}) copy-start(bf16[32,512]{1,0:T(8,128)(2,1)} %param.17) | copy-start | bytes 98308
  7.2 13.6 %copy-start.5 = (bf16[32,512]{1,0:T(8,128)(2,1)S(1)}, bf16[32,512]{1,0:T(8,128)(2,1)}, u32[]{:S(2)}) copy-start(bf16[32,512]{1,0:T(8,128)(2,1)} %param.19) | copy-start | bytes 98308
  19.1 2.1 copy-start.9
  19.5 2.6 %copy-start.10 = (bf16[32,4]{0,1:T(4,128)(2,1)S(1)}, bf16[32,4]{0,1:T(4,128)(2,1)}, u32[]{:S(2)}) copy-start(bf16[32,4]{0,1:T(4,128)(2,1)} %param.21) | copy-start | bytes 772
  25.2 13.3 %copy-start.4 = (bf16[64,2048]{1,0:T(8,128)(2,1)S(1)}, bf16[64,2048]{1,0:T(8,128)(2,1)}, u32[]{:S(2)}) copy-start(bf16[64,2048]{1,0:T(8,128)(2,1)} %param.27) | copy-start | bytes 786436
  25.2 13.4 %copy-start.3 = (bf16[2048,64]{0,1:T(8,128)(2,1)S(1)}, bf16[2048,64]{0,1:T(8,128)(2,1)}, u32[]{:S(2)}) copy-start(bf16[2048,64]{0,1:T(8,128)(2,1)} %param.26) | copy-start | bytes 786436
  25.2 56.9 %all-to-all-start.1 = ((bf16[64,3,1545]{2,1,0:T(4,128)(2,1)}), bf16[64,3,1545]{2,1,0:T(4,128)(2,1)S(1)}, u32[]{:S(2)}, u32[]{:S(2)}) async-start(bf16[64,3,1545]{2,1,0:T(4,128)(2,1)} %concatenate.33), calls=%async_computation.1 | async-start | bytes 1703936 | tf_op jit(solution)/shard_map/all_to_all | solution.py:36
  38.5 56.7 %all-reduce.3.cloned.1.call-start = ((), (), s32[]{:S(2)}) async-start(), calls=%async_computation.8 | async-start | bytes 2101248
  38.5 2.5 %copy-start.8 = (bf16[16]{0:T(256)(128)(2,1)S(1)}, bf16[16]{0:T(256)(128)(2,1)}, u32[]{:S(2)}) copy-start(bf16[16]{0:T(256)(128)(2,1)} %param.25) | copy-start | bytes 100
  41.2 6.0 %copy-start.11 = (bf16[128]{0:T(256)(128)(2,1)S(1)}, bf16[128]{0:T(256)(128)(2,1)}, u32[]{:S(2)}) copy-start(bf16[128]{0:T(256)(128)(2,1)} %param.23) | copy-start | bytes 772
  41.2 6.0 %copy-start.12 = (f32[4]{0:T(128)S(1)}, f32[4]{0:T(128)}, u32[]{:S(2)}) copy-start(f32[4]{0:T(128)} %param.22) | copy-start | bytes 52
  46.1 1.0 copy-start.1
  46.1 37.6 %copy-start.2 = (f32[3,4,128,128]{3,2,1,0:T(8,128)S(1)}, f32[3,4,128,128]{3,2,1,0:T(8,128)}, u32[]{:S(2)}) copy-start(f32[3,4,128,128]{3,2,1,0:T(8,128)} %param.15) | copy-start | bytes 2359300
  86.6 27.8 %all-to-all-start.2 = ((bf16[64,3,512]{2,1,0:T(4,128)(2,1)}), bf16[64,3,512]{2,1,0:T(4,128)(2,1)S(1)}, u32[]{:S(2)}, u32[]{:S(2)}) async-start(bf16[64,3,512]{2,1,0:T(4,128)(2,1)} %broadcast_in_dim.2), calls=%async_computation.2 | async-start | bytes 524288 | tf_op jit(solution)/shard_map/all_to_all | solution.py:54
  95.2 19.3 %copy-start.6 = (bf16[512,32]{0,1:T(8,128)(2,1)S(1)}, bf16[512,32]{0,1:T(8,128)(2,1)}, u32[]{:S(2)}) copy-start(bf16[512,32]{0,1:T(8,128)(2,1)} %param.24) | copy-start | bytes 98308
  95.2 27.3 %copy-start.7 = (bf16[192,16]{0,1:T(8,128)(2,1)S(1)}, bf16[192,16]{0,1:T(8,128)(2,1)}, u32[]{:S(2)}) copy-start(bf16[192,16]{0,1:T(8,128)(2,1)} %param.14) | copy-start | bytes 18436
  127.3 35.8 %all-to-all-start.5 = ((bf16[64,32,97]{2,1,0:T(8,128)(2,1)}), bf16[64,32,97]{2,1,0:T(8,128)(2,1)S(1)}, u32[]{:S(2)}, u32[]{:S(2)}) async-start(bf16[64,32,97]{2,1,0:T(8,128)(2,1)} %stack.8), calls=%async_computation.5 | async-start | bytes 1048576 | tf_op jit(solution)/shard_map/all_to_all | solution.py:13
Sparse Core Ops, SparseCore 0:
  47.3 42.8 all-reduce.2
